TPU v7x, 32 devices: a whole 2x2x4 slice. The times are simulated.
32 devices in a mesh: sp: 8 (over z, y), tp: 4 (over x, core).
Axes of the slice: x: 2, y: 2, z: 4, core: 2. Of those that a mesh axis runs over, the one named last changes fastest.
Arguments:
- stream: bfloat16 [3072, 2048], P(('sp', 'tp')), may hold values from -6 to 6
- query_nope: bfloat16 [3072, 16, 128], P('sp', 'tp'), may hold values from -6 to 6
- query_rope: bfloat16 [3072, 16, 64], P('sp', 'tp'), may hold values from -700 to 700
- latent: bfloat16 [3072, 512], P('sp'), may hold values from -6 to 6
- rope_key: bfloat16 [3072, 64], P('sp'), may hold values from -6 to 6
- latent_gain: float32 [512], replicated, may hold values from 0.1 to 1.9
- key_up: bfloat16 [512, 16, 128], P(None, 'tp'), may hold values from -0.375 to 0.375
- value_up: bfloat16 [512, 16, 128], P(None, 'tp'), may hold values from -2.6516504 to 2.6516504
- out_gain: float32 [2048], P('tp'), may hold values from 0.1 to 1.9
- out_weight: bfloat16 [2048, 2048], P('tp'), may hold values from -0.125 to 0.125
- norm_gain: float32 [2048], replicated, may hold values from 0.1 to 1.9
- ff_in: bfloat16 [2048, 8192], P('sp', 'tp'), may hold values from -0.125 to 0.125
- ff_out: bfloat16 [8192, 2048], P('tp', 'sp'), may hold values from -0.0625 to 0.0625
Outputs:
- layer_out: bfloat16 [3072, 2048], P(('sp', 'tp'))
All inputs are finite; a program needn't handle non-finite values.
Results may differ from a plain program's by a relative error of at most 0.018.
Values may be sent and summed in bfloat16 or wider, within the bound.
A program may use at most 128 MiB of HBM per device.

v0:
```python
import functools
import math

import jax
import jax.numpy as jnp
from jax import lax
from jax.experimental import pallas as pl
from jax.experimental.pallas import tpu as pltpu
from jax.sharding import PartitionSpec as P

EPS = 1e-06
THETA = 10000.0
F32 = jnp.float32
BF16 = jnp.bfloat16
MESH = pl.DeviceIdType.MESH
LANES = 128
SUBS = 4


def turn(values, positions):
    full_width = values.shape[-1]
    half_width = full_width // 2
    inverse = jnp.power(THETA, -jnp.arange(0, full_width, 2, dtype=F32) / full_width)
    angles = positions[:, None] * inverse[None, :]
    cosine = jnp.cos(angles)
    sine_part = jnp.sin(angles)
    if values.ndim == 3:
        cosine = cosine[:, None, :]
        sine_part = sine_part[:, None, :]
    vector = values.astype(F32)
    lower_half = vector[..., :half_width]
    upper_half = vector[..., half_width:]
    return jnp.concatenate(
        [
            lower_half * cosine - upper_half * sine_part,
            lower_half * sine_part + upper_half * cosine,
        ],
        axis=-1,
    )


def ring_shape(n):
    rows = 1
    while rows * rows < n:
        rows *= 2
    return (rows, n // rows) if n % rows == 0 else (n, 1)


def ring_pos(n, index):
    nz, ny = ring_shape(n)
    if ny == 1:
        return index
    z, y = index // ny, index % ny
    r = nz - 1 - z
    odd = r % 2
    c = (1 - odd) * (y - 1) + odd * (ny - 1 - y)
    return jnp.where(y == 0, z, nz + r * (ny - 1) + c)


def ring_at(n, pos):
    nz, ny = ring_shape(n)
    if ny == 1:
        return pos
    q = jnp.maximum(pos - nz, 0)
    r, c = q // (ny - 1), q % (ny - 1)
    odd = r % 2
    y = 1 + (1 - odd) * c + odd * (ny - 2 - c)
    return jnp.where(pos < nz, pos * ny, (nz - 1 - r) * ny + y)


def kernel(
    n, tp, heads, latent_width, width,
    kv_ref, q_ref, vup_ref, gain_ref, ow_ref, stream_ref, ngain_ref, ffin_ref, ffout_ref,
    out_ref,
    kv, fi, fo, ow, sc, acc, gated, proj, red, sq_out, sq_in, mid, xs, act, mixed, mix_out, mix_in,
    local_sem, lat_send, lat_recv, par_send, par_recv, w_send, w_recv,
    t_send, t_recv, m_send, m_recv,
):
    sp = lax.axis_index("sp")
    me = lax.axis_index("tp")
    pos = ring_pos(n, sp)
    rows = stream_ref.shape[0] * tp
    share = rows // tp
    total = width
    hidden = act.shape[1]
    dblk = total // n
    keys = kv.shape[0]
    core = me % 2
    partner = me + 1 - 2 * core

    def at(offset):
        return ring_at(n, lax.rem(pos + offset + n, n))

    right, left = at(1), at(-1)
    towards = (right, left)

    def peer(j):
        return lax.rem(me + j, tp)

    local = [
        pltpu.make_async_copy(ffin_ref, fi.at[pl.ds(sp * dblk, dblk)], local_sem.at[0]),
        pltpu.make_async_copy(ffout_ref, fo.at[sp], local_sem.at[1]),
        pltpu.make_async_copy(ow_ref, ow, local_sem.at[2]),
        pltpu.make_async_copy(kv_ref, kv.at[pl.ds(sp * rows, rows)], local_sem.at[3]),
    ]
    for c in (3, 0, 1, 2):
        local[c].start()

    barrier = pltpu.get_barrier_semaphore()
    for d in towards:
        pl.semaphore_signal(barrier, inc=1, device_id=(d, me), device_id_type=MESH)
    for j in range(1, tp):
        pl.semaphore_signal(barrier, inc=1, device_id=(sp, peer(j)), device_id_type=MESH)
    pl.semaphore_wait(barrier, tp + 1)

    quarter = rows // 4

    def lat_piece(src, way, c):
        return kv.at[pl.ds(src * rows + (2 * c + way) * quarter, quarter)]

    def came(way, step):
        return at(-1 - step) if way == 0 else at(1 + step)

    def going(way, step):
        return at(-step) if way == 0 else at(step)

    def lat_copy(way, step):
        ref = lat_piece(going(way, step), way, core)
        return pltpu.make_async_remote_copy(
            ref, ref, lat_send.at[way, step], lat_recv.at[way, step],
            device_id=(towards[way], me), device_id_type=MESH)

    def lat_wait(way, step):
        ref = lat_piece(came(way, step), way, core)
        pltpu.make_async_remote_copy(
            ref, ref, lat_send.at[way, step], lat_recv.at[way, step],
            device_id=(towards[way], me), device_id_type=MESH).wait_recv()

    def par_copy(way, step, c):
        ref = lat_piece(came(way, step), way, c)
        return pltpu.make_async_remote_copy(
            ref, ref, par_send.at[way, step], par_recv.at[way, step],
            device_id=(sp, partner), device_id_type=MESH)

    def w_piece(buf, src, way, sub):
        if buf == 0:
            part = dblk // (2 * SUBS)
            return fi.at[pl.ds(src * dblk + (SUBS * way + sub) * part, part)]
        part = hidden // (2 * SUBS)
        return fo.at[src, pl.ds((SUBS * way + sub) * part, part)]

    def w_copy(buf, way, sub, step):
        ref = w_piece(buf, going(way, step), way, sub)
        return pltpu.make_async_remote_copy(
            ref, ref, w_send.at[buf, way, sub, step], w_recv.at[buf, way, sub, step],
            device_id=(towards[way], me), device_id_type=MESH)

    def w_wait(buf, way, sub, step):
        ref = w_piece(buf, came(way, step), way, sub)
        pltpu.make_async_remote_copy(
            ref, ref, w_send.at[buf, way, sub, step], w_recv.at[buf, way, sub, step],
            device_id=(towards[way], me), device_id_type=MESH).wait_recv()

    units = [(b, s, u) for b in range(2) for s in range(n - 1) for u in range(SUBS)]
    ff_in_units = (n - 1) * SUBS
    cursor = [0]
    waited = set()

    def need(buf, step, sub):
        if (buf, step, sub) not in waited:
            waited.add((buf, step, sub))
            for way in range(2):
                w_wait(buf, way, sub, step)

    def advance(until):
        while cursor[0] < min(until, len(units)):
            buf, step, sub = units[cursor[0]]
            if step > 0:
                need(buf, step - 1, sub)
            for way in range(2):
                w_copy(buf, way, sub, step).start()
            cursor[0] += 1

    def one_more(limit):
        if cursor[0] < limit:
            advance(cursor[0] + 1)

    local[3].wait()
    for way in range(2):
        lat_copy(way, 0).start()
    local[0].wait()
    advance(1)
    for step in range(n - 1):
        for way in range(2):
            lat_wait(way, step)
            if step < n - 2:
                lat_copy(way, step + 1).start()
            par_copy(way, step, core).start()
        one_more(ff_in_units)
    for step in range(n - 1):
        for way in range(2):
            par_copy(way, step, 1 - core).wait_recv()

    scale = 1.0 / math.sqrt(LANES + (q_ref.shape[2] - latent_width) // 2)
    chunk = sc.shape[2]
    chunks = keys // chunk
    vdim = LANES
    squares = jnp.zeros((rows, 1), F32)
    for h in range(heads):
        def score(c, top):
            s = lax.dot_general(
                q_ref[h], kv[pl.ds(c * chunk, chunk), :], (((1,), (1,)), ((), ())),
                preferred_element_type=F32) * scale
            sc[c] = s
            return jnp.maximum(top, jnp.max(s, axis=1, keepdims=True))

        top = lax.fori_loop(0, chunks, score, jnp.full((rows, 1), -jnp.inf, F32))
        one_more(ff_in_units)
        acc[...] = jnp.zeros_like(acc)

        def gather(c, den):
            e = jnp.exp(sc[c] - top)
            acc[...] += jnp.dot(
                e.astype(BF16), kv[pl.ds(c * chunk, chunk), pl.ds(0, latent_width)],
                preferred_element_type=F32)
            return den + jnp.sum(e, axis=1, keepdims=True)

        den = lax.fori_loop(0, chunks, gather, jnp.zeros((rows, 1), F32))
        lat = (acc[...] / den).astype(BF16)
        one = jnp.dot(lat, vup_ref[:, h * vdim:(h + 1) * vdim], preferred_element_type=F32)
        squares = squares + jnp.sum(one * one, axis=1, keepdims=True)
        gated[:, h * vdim:(h + 1) * vdim] = (one * gain_ref[:, h * vdim:(h + 1) * vdim]).astype(BF16)
        one_more(ff_in_units)
    sq_out[...] = jnp.broadcast_to(squares, sq_out.shape)
    local[2].wait()

    tile = total // 4

    def project(c):
        cols = pl.ds(pl.multiple_of(c * tile, tile), tile)
        proj[:, cols] = jnp.dot(gated[...], ow[:, cols], preferred_element_type=F32).astype(BF16)

    pl.loop(0, 2)(project)
    one_more(ff_in_units)
    pl.loop(2, 4)(project)

    def block(owner):
        return pl.ds(owner * share, share)

    def t_copy(kind, j, out):
        other = peer(j) if out else me
        mine = me if out else peer(tp - j)
        if kind == 0:
            a, b = sq_out.at[block(other)], sq_in.at[mine]
        elif kind == 1:
            a, b = proj.at[block(other)], red.at[mine]
        else:
            a = b = xs.at[block(mine)]
        return pltpu.make_async_remote_copy(
            a, b, t_send.at[kind, j], t_recv.at[kind, j],
            device_id=(sp, peer(j)), device_id_type=MESH)

    for j in range(1, tp):
        t_copy(0, j, True).start()
        t_copy(1, j, True).start()
    advance(ff_in_units - SUBS - 2)
    for j in range(1, tp):
        t_copy(0, j, False).wait_recv()
        t_copy(1, j, False).wait_recv()
    summed = proj[block(me), :].astype(F32)
    square = sq_out[block(me), :]
    for j in range(1, tp):
        summed = summed + red[peer(tp - j)].astype(F32)
        square = square + sq_in[peer(tp - j)]
    row_scale = lax.rsqrt(square[:, :1] / (heads * tp * vdim) + EPS)
    middle = stream_ref[...].astype(F32) + row_scale * summed
    mid[...] = middle
    norm = lax.rsqrt(jnp.mean(middle * middle, axis=1, keepdims=True) + EPS)
    xs[block(me), :] = (middle * norm * ngain_ref[...]).astype(BF16)
    for j in range(1, tp):
        t_copy(2, j, True).start()
    local[1].wait()
    advance(ff_in_units + SUBS)
    for sub in range(SUBS):
        need(0, n - 2, sub)
    for j in range(1, tp):
        t_copy(2, j, False).wait_recv()

    wide = 512 if hidden % 512 == 0 else 128

    def first(c):
        cols = pl.ds(c * wide, wide)
        pre = jnp.dot(xs[...], fi[:, cols], preferred_element_type=F32)
        pre = jnp.maximum(pre, 0.0)
        act[:, cols] = (pre * pre).astype(BF16)

    for c in range(hidden // wide):
        first(c)
        one_more(len(units))

    mixed[sp] = jnp.dot(act[...], fo[sp], preferred_element_type=F32)
    half = hidden // 2

    def part(src, way):
        return jnp.dot(act[:, way * half:(way + 1) * half], fo[src, way * half:(way + 1) * half],
                       preferred_element_type=F32)

    def m_copy(order, src, j, out):
        other = peer(j) if out else me
        mine = me if out else peer(tp - j)
        return pltpu.make_async_remote_copy(
            mix_out.at[src, block(other)], mix_in.at[mine, src],
            m_send.at[order, j], m_recv.at[order, j],
            device_id=(sp, peer(j)), device_id_type=MESH)

    finished = []
    seen = set()

    def finish(offset, src):
        order = len(finished)
        finished.append(src)
        mix_out[src] = mixed[src].astype(BF16)
        for j in range(1, tp):
            m_copy(order, src, j, True).start()

    for step in range(n - 1):
        advance(ff_in_units + (step + 2) * SUBS)
        for sub in range(SUBS):
            need(1, step, sub)
        for way in range(2):
            offset = (-1 - step) % n if way == 0 else (1 + step) % n
            src = came(way, step)
            if offset in seen:
                mixed[src] += part(src, way)
                finish(offset, src)
            else:
                seen.add(offset)
                mixed[src] = part(src, way)
        if step == 0:
            finish(0, sp)

    for order, src in enumerate(finished):
        cols = pl.ds(pl.multiple_of(src * dblk, dblk), dblk)
        whole = mix_out[src, block(me), :].astype(F32)
        for j in range(1, tp):
            m_copy(order, src, j, False).wait_recv()
            whole = whole + mix_in[peer(tp - j), src].astype(F32)
        out_ref[:, cols] = (mid[:, cols] + whole).astype(BF16)

    for step in range(n - 1):
        for way in range(2):
            lat_copy(way, step).wait_send()
            par_copy(way, step, core).wait_send()
            for buf in range(2):
                for sub in range(SUBS):
                    w_copy(buf, way, sub, step).wait_send()
    for j in range(1, tp):
        for kind in range(3):
            t_copy(kind, j, True).wait_send()
        for order, src in enumerate(finished):
            m_copy(order, src, j, True).wait_send()


def body(
    n, tp,
    stream, query_nope, query_rope, latent, rope_key, latent_gain,
    key_up, value_up, out_gain, out_weight, norm_gain, ff_in, ff_out,
):
    rows, heads = query_nope.shape[:2]
    width = stream.shape[1]
    latent_width = latent.shape[1]
    rope = rope_key.shape[1]
    pad = -rope % LANES
    dblk, hidden = ff_in.shape
    share = rows // tp
    positions = (lax.axis_index("sp") * rows + jnp.arange(rows, dtype=jnp.int32)).astype(F32)
    lat_full = latent.astype(F32)
    normed = (
        lat_full
        * lax.rsqrt(jnp.mean(lat_full * lat_full, axis=-1, keepdims=True) + EPS)
        * latent_gain
    ).astype(BF16)
    keys_rot = turn(rope_key, positions).astype(BF16)
    query_rot = turn(query_rope, positions).astype(BF16)
    query_lat = jnp.einsum(
        "thn,lhn->htl", query_nope, key_up, preferred_element_type=F32
    ).astype(BF16)
    kv = jnp.concatenate([normed, keys_rot, jnp.zeros((rows, pad), BF16)], axis=1)
    q = jnp.concatenate(
        [query_lat, query_rot.transpose(1, 0, 2), jnp.zeros((heads, rows, pad), BF16)], axis=2
    )
    keys = n * rows
    chunk = 2 * rows if n % 2 == 0 else rows
    vm = pl.BlockSpec(memory_space=pltpu.VMEM)
    hbm = pl.BlockSpec(memory_space=pl.ANY)
    dma = pltpu.SemaphoreType.DMA
    return pl.pallas_call(
        functools.partial(kernel, n, tp, heads, latent_width, width),
        out_shape=jax.ShapeDtypeStruct((share, width), BF16),
        in_specs=[hbm, vm, vm, vm, hbm, vm, vm, hbm, hbm],
        out_specs=vm,
        scratch_shapes=[
            pltpu.VMEM((keys, kv.shape[1]), BF16),
            pltpu.VMEM((width, hidden), BF16),
            pltpu.VMEM((n, hidden, dblk), BF16),
            pltpu.VMEM(out_weight.shape, BF16),
            pltpu.VMEM((keys // chunk, rows, chunk), F32),
            pltpu.VMEM((rows, latent_width), F32),
            pltpu.VMEM((rows, out_weight.shape[0]), BF16),
            pltpu.VMEM((rows, width), BF16),
            pltpu.VMEM((tp, share, width), BF16),
            pltpu.VMEM((rows, LANES), F32),
            pltpu.VMEM((tp, share, LANES), F32),
            pltpu.VMEM((share, width), F32),
            pltpu.VMEM((rows, width), BF16),
            pltpu.VMEM((rows, hidden), BF16),
            pltpu.VMEM((n, rows, dblk), F32),
            pltpu.VMEM((n, rows, dblk), BF16),
            pltpu.VMEM((tp, n, share, dblk), BF16),
            dma((4,)),
            dma((2, n - 1)), dma((2, n - 1)), dma((2, n - 1)), dma((2, n - 1)),
            dma((2, 2, SUBS, n - 1)), dma((2, 2, SUBS, n - 1)),
            dma((3, tp)), dma((3, tp)),
            dma((n, tp)), dma((n, tp)),
        ],
        compiler_params=pltpu.CompilerParams(
            collective_id=0, has_side_effects=True, vmem_limit_bytes=63 * 1024 * 1024
        ),
    )(
        kv, q, value_up.reshape(latent_width, -1), out_gain[None, :], out_weight,
        stream, norm_gain[None, :], ff_in, ff_out,
    )


def solution(mesh):
    placed = (
        P(("sp", "tp"), None),
        P("sp", "tp", None),
        P("sp", "tp", None),
        P("sp", None),
        P("sp", None),
        P(),
        P(None, "tp", None),
        P(None, "tp", None),
        P("tp"),
        P("tp", None),
        P(),
        P("sp", "tp"),
        P("tp", "sp"),
    )
    return jax.shard_map(
        functools.partial(body, mesh.shape["sp"], mesh.shape["tp"]),
        mesh=mesh, in_specs=placed, out_specs=P(("sp", "tp"), None), check_vma=False
    )
```

profile of v0, /device:TPU:0, one launch (start us, length us, event | category | flops | bytes accessed | tf_op | source)
XLA Modules:
  0.0 203.9 jit_solution(15027641247898533442)
XLA Ops:
  0.0 0.0 copy-start
  0.0 1.0 copy.18
  1.0 0.8 multiply_cosine_fusion
  1.9 1.2 copy.22
  3.0 0.1 convert_element_type.29
  3.1 0.0 copy-start.3
  3.1 0.4 subtract_convert_fusion
  3.5 0.2 maximum_bitcast_fusion
  3.7 0.1 pad.8.clone
  3.8 0.0 copy-done
  3.8 0.3 copy-done.3
  4.1 0.6 convolution_convert_fusion
  4.7 0.0 copy-start.1
  4.7 0.0 copy-start.4
  4.7 1.7 maximum_maximum_fusion.q_ref
  6.4 0.0 copy-done.1
  6.4 0.2 fusion
  6.6 0.0 copy-done.4
  6.6 0.2 fusion.2
  6.7 0.9 maximum_maximum_fusion.1.kv_ref
  7.7 0.0 copy-done.2
  7.7 0.9 copy.29
  8.5 193.6 %shard_map.127 = bf16[96,2048]{1,0:T(8,128)(2,1)} custom-call(bf16[384,640]{1,0:T(8,128)(2,1)} %maximum_maximum_fusion.1.kv_ref, bf16[4,384,640]{2,1,0:T(8,128)(2,1)} %maximum_maximum_fusion.q_ref, bf16[512,512]{1,0:T(8,128)(2,1)} %bitcast.8, f32[1,512]{1,0:T(1,128)} %bitcast.11, bf16[512,2048]{1,0:T(8,128)(2,1)} %ow_ref.1, bf16[96,2048]{1,0:T(8,128)(2,1)} %stream_ref.1, ...), custom_call_target="tpu_custom_call" | custom-call | tf_op jit(solution)/shard_map/pallas_call | solution.py:397
  202.2 1.8 copy.31
  (6 shorter events, 0.0 us)
Async XLA Ops:
  0.0 3.8 %copy-start = (bf16[512,4,128]{2,1,0:T(4,128)(2,1)S(1)}, bf16[512,4,128]{2,1,0:T(4,128)(2,1)}, u32[]{:S(2)}) copy-start(bf16[512,4,128]{2,1,0:T(4,128)(2,1)} %param.19) | copy-start | bytes 1572868
  3.1 1.0 copy-start.3
  4.7 1.7 copy-start.1
  4.7 1.9 copy-start.4
  6.4 1.3 copy-start.2
where the time goes:
time: 204 us
  Pallas kernels  194 us (95%)
  local copies, waits for them, and re-layouts  5.15 us (3%)
  other arithmetic  4.46 us (2%)
    pallas_call x1, Pallas kernels, body(): pl.pallas_call(functools.partial(kernel, n, tp, heads, latent_width, widt...  194 us
    unnamed x14, local copies, waits for them, and re-layouts  5.07 us

commit v1 on v0

v1 whole, which is shorter than its diff:
```python
import functools
import math

import jax
import jax.numpy as jnp
from jax import lax
from jax.experimental import pallas as pl
from jax.experimental.pallas import tpu as pltpu
from jax.sharding import PartitionSpec as P

EPS = 1e-06
THETA = 10000.0
F32 = jnp.float32
BF16 = jnp.bfloat16
MESH = pl.DeviceIdType.MESH
LANES = 128


def turn(values, positions):
    full_width = values.shape[-1]
    half_width = full_width // 2
    inverse = jnp.power(THETA, -jnp.arange(0, full_width, 2, dtype=F32) / full_width)
    angles = positions[:, None] * inverse[None, :]
    cosine = jnp.cos(angles)
    sine_part = jnp.sin(angles)
    if values.ndim == 3:
        cosine = cosine[:, None, :]
        sine_part = sine_part[:, None, :]
    vector = values.astype(F32)
    lower_half = vector[..., :half_width]
    upper_half = vector[..., half_width:]
    return jnp.concatenate(
        [
            lower_half * cosine - upper_half * sine_part,
            lower_half * sine_part + upper_half * cosine,
        ],
        axis=-1,
    )


def ring_shape(n):
    rows = 1
    while rows * rows < n:
        rows *= 2
    return (rows, n // rows) if n % rows == 0 else (n, 1)


def ring_pos(nz, ny, index):
    if ny == 1:
        return index
    z, y = lax.div(index, ny), lax.rem(index, ny)
    r = nz - 1 - z
    odd = lax.rem(r, 2)
    c = (1 - odd) * (y - 1) + odd * (ny - 1 - y)
    return jnp.where(y == 0, z, nz + r * (ny - 1) + c)


def ring_at(nz, ny, pos):
    if ny == 1:
        return pos
    q = jnp.maximum(pos - nz, 0)
    r, c = lax.div(q, ny - 1), lax.rem(q, ny - 1)
    odd = lax.rem(r, 2)
    y = 1 + (1 - odd) * c + odd * (ny - 2 - c)
    return jnp.where(pos < nz, pos * ny, (nz - 1 - r) * ny + y)


def flip(index, bits):
    bit = 1
    out = index
    while bit <= bits:
        if bits & bit:
            out = out + bit * (1 - 2 * lax.rem(lax.div(index, bit), 2))
        bit *= 2
    return out


def kernel(
    n, tp, heads, latent_width, width,
    kv_ref, q_ref, vup_ref, gain_ref, ow_ref, stream_ref, ngain_ref, ffin_ref, ffout_ref,
    out_ref,
    kv, fi, fo, ow, sc, top, acc, gated, pout, pin, keep, xout, xin, sq_out, sq_in, mid, xs, act,
    fresh, mixed, mpo, mpi, mxo, mxi, mzo, mzi,
    local_sem, ka_send, ka_recv, kx_send, kx_recv, kp_send, kp_recv,
    c_send, c_recv, w_send, w_recv,
    s_send, s_recv, r_send, r_recv, g_send, g_recv,
    mp_send, mp_recv, mx_send, mx_recv, mz_send, mz_recv,
):
    sp = lax.axis_index("sp")
    me = lax.axis_index("tp")
    nz, ny = ring_shape(n)
    hz, m, nx = nz // 2, n // 2, tp // 2
    z, y = lax.div(sp, ny), lax.rem(sp, ny)
    x, core = lax.div(me, 2), lax.rem(me, 2)
    half, local = lax.div(sp, m), lax.rem(sp, m)
    zl = lax.div(local, ny)
    mate = lax.rem(sp + m, n)
    pcore = me + 1 - 2 * core
    rows = q_ref.shape[1]
    share = rows // tp
    dblk = width // n
    hh = act.shape[2]
    chunk = sc.shape[3]
    vdim = LANES
    pos = ring_pos(hz, ny, local)

    def at(offset):
        return half * m + ring_at(hz, ny, lax.rem(pos + offset + m, m))

    turnway = lax.rem(pos, 2)

    def space(kz, ky):
        return flip(z, kz) * ny + flip(y, ky)

    def along(kx, c):
        return flip(x, kx) * 2 + c

    sends = []

    def remote(a, b, s, r, to, when=None):
        cp = pltpu.make_async_remote_copy(a, b, s, r, device_id=to, device_id_type=MESH)
        cp.start()
        sends.append(cp)

    def arrived(ref, s, r):
        pltpu.make_async_remote_copy(
            ref, ref, s, r, device_id=(sp, pcore), device_id_type=MESH).wait_recv()

    def lanes(h):
        return pl.ds(pl.multiple_of(h * hh, LANES), hh)

    def deep(h):
        return pl.ds(pl.multiple_of(h * hh, LANES), hh)

    def block_rows(s):
        return pl.ds(pl.multiple_of(s * dblk, dblk), dblk)

    own = [
        pltpu.make_async_copy(kv_ref, kv.at[pl.ds(sp * rows, rows)], local_sem.at[0]),
        pltpu.make_async_copy(ffin_ref.at[:, lanes(half)], fi.at[block_rows(sp)], local_sem.at[1]),
        pltpu.make_async_copy(ffout_ref.at[deep(half)], fo.at[sp], local_sem.at[2]),
        pltpu.make_async_copy(ow_ref, ow, local_sem.at[3]),
    ]
    for cp in own:
        cp.start()

    barrier = pltpu.get_barrier_semaphore()
    for i in range(1, n):
        pl.semaphore_signal(
            barrier, inc=1, device_id=(lax.rem(sp + i, n), me), device_id_type=MESH)
    for j in range(1, tp):
        pl.semaphore_signal(
            barrier, inc=1, device_id=(sp, lax.rem(me + j, tp)), device_id_type=MESH)
    pl.semaphore_wait(barrier, n + tp - 2)

    def piece(s, t):
        return kv.at[pl.ds(pl.multiple_of(s * rows + t * share, share), share)]

    def arrive(kz, ky):
        ref = piece(space(kz, ky), me)
        i = kz * ny + ky
        arrived(ref, ka_send.at[i], ka_recv.at[i])
        if ky == 0:
            for k in range(1, ny):
                j = kz * ny + k
                remote(ref, ref, ka_send.at[j], ka_recv.at[j], (space(0, k), me))
        for kx in range(1, nx):
            remote(ref, ref, kx_send.at[i, kx], kx_recv.at[i, kx], (sp, along(kx, core)))
        remote(ref, ref, kp_send.at[i, 0], kp_recv.at[i, 0], (sp, pcore))

    def across(kz, ky):
        i = kz * ny + ky
        for kx in range(1, nx):
            ref = piece(space(kz, ky), along(kx, core))
            arrived(ref, kx_send.at[i, kx], kx_recv.at[i, kx])
            remote(ref, ref, kp_send.at[i, kx], kp_recv.at[i, kx], (sp, pcore))

    def settle(kz, ky):
        i = kz * ny + ky
        for kx in range(nx):
            ref = piece(space(kz, ky), along(kx, 1 - core))
            arrived(ref, kp_send.at[i, kx], kp_recv.at[i, kx])

    def inner_of(h):
        return (hz - 1) * (1 - h)

    def is_inner(hm):
        return lax.div(lax.rem(hm, m), ny) == inner_of(half)

    def w_whole(b, s):
        return fi.at[block_rows(s)] if b == 0 else fo.at[s]

    def w_ref(b, s, way):
        if b == 0:
            return fi.at[pl.ds(pl.multiple_of(s * dblk + way * (dblk // 2), dblk // 2), dblk // 2)]
        return fo.at[s, pl.ds(pl.multiple_of(way * (hh // 2), hh // 2), hh // 2)]

    def home(way, step):
        return at((2 * way - 1) * step)

    def source(g, hm):
        if g == 0:
            return hm
        return (1 - half) * m + (g - 1) * ny + lax.rem(hm, ny)

    def cross(b):
        to = (1 - half) * m + inner_of(1 - half) * ny + y
        a = ffin_ref.at[:, lanes(1 - half)] if b == 0 else ffout_ref.at[deep(1 - half)]
        remote(a, w_whole(b, sp), c_send.at[b], c_recv.at[b, zl], (to, me))

    guarded = []

    def unit(b, g, step, k):
        way = turnway if k == 0 else 1 - turnway
        hm = home(way, step)
        s = source(g, hm)
        ref = w_ref(b, s, way)
        cp = pltpu.make_async_remote_copy(
            ref, ref, w_send.at[b, g, way, step], w_recv.at[b, g, way, step],
            device_id=(at(1 - 2 * way), me), device_id_type=MESH)

        def go():
            if step > 0:
                arrived(ref, w_send.at[b, g, way, step - 1], w_recv.at[b, g, way, step - 1])
            elif g > 0 and k == 0:
                arrived(w_whole(b, s), c_send.at[b], c_recv.at[b, g - 1])
            if step < m - 1:
                cp.start()

        if g == 0:
            go()
            if step < m - 1:
                sends.append(cp)
        else:
            pl.when(is_inner(hm))(go)
            if step < m - 1:
                guarded.append((hm, cp))

    others = range(1, hz + 1)
    issued = set()

    def do(b, g, step, k):
        if step < m and (b, g, step, k) not in issued:
            if step > 0:
                do(b, g, step - 1, k)
            issued.add((b, g, step, k))
            unit(b, g, step, k)

    def near(b, step, *ks):
        for k in ks:
            do(b, 0, step, k)

    def far(b, step, *ks):
        for k in ks:
            for g in others:
                do(b, g, step, k)

    own[0].wait()
    mine = piece(sp, me)
    for ky in range(1, ny):
        remote(mine, mine, ka_send.at[ky], ka_recv.at[ky], (space(0, ky), me))
    for kz in range(1, nz):
        remote(mine, mine, ka_send.at[kz * ny], ka_recv.at[kz * ny], (space(kz, 0), me))
    own[1].wait()
    near(0, 0, 0, 1)

    scale = 1.0 / math.sqrt(LANES + (q_ref.shape[2] - latent_width) // 2)

    def score(kz):
        keys = pl.ds(pl.multiple_of(flip(z, kz) * chunk, chunk), chunk)

        def one(h, _):
            s = lax.dot_general(
                q_ref[h], kv[keys, :], (((1,), (1,)), ((), ())),
                preferred_element_type=F32) * scale
            sc[kz, h] = s
            best = jnp.max(s, axis=1, keepdims=True)
            if kz > 0:
                best = jnp.maximum(best, top[h][:, :1])
            top[h] = jnp.broadcast_to(best, (rows, LANES))
            return 0

        lax.fori_loop(0, heads, one, 0)

    for ky in range(1, ny):
        arrive(0, ky)
    arrive(1, 0)
    for ky in range(1, ny):
        across(0, ky)
    for kz in range(2, nz):
        arrive(kz, 0)
    own[2].wait()
    cross(0)
    near(1, 0, 0, 1)
    for ky in range(1, ny):
        settle(0, ky)
    for ky in range(1, ny):
        arrive(1, ky)
    score(0)
    for kz in range(1, nz):
        for ky in range(1, ny):
            if kz > 1:
                arrive(kz, ky)
    near(0, 1, 0)
    for kz in range(1, nz):
        for ky in range(ny):
            across(kz, ky)
        for ky in range(ny):
            settle(kz, ky)
        score(kz)
        if kz == 1:
            cross(1)
            near(1, 1, 0)
            near(0, 1, 1)
        elif kz == nz - 1:
            far(0, 0, 0, 1)

    squares = jnp.zeros((rows, 1), F32)
    for h in range(heads):
        peak = top[h][:, :1]
        acc[...] = jnp.zeros_like(acc)

        def gather(kz, den):
            zk = flip(z, 0)
            zk = jnp.where(kz == 0, z, zk)
            for k in range(1, nz):
                zk = jnp.where(kz == k, flip(z, k), zk)
            e = jnp.exp(sc[kz, h] - peak)
            acc[...] += jnp.dot(
                e.astype(BF16),
                kv[pl.ds(pl.multiple_of(zk * chunk, chunk), chunk), pl.ds(0, latent_width)],
                preferred_element_type=F32)
            return den + jnp.sum(e, axis=1, keepdims=True)

        den = lax.fori_loop(0, nz, gather, jnp.zeros((rows, 1), F32))
        lat = (acc[...] / den).astype(BF16)
        cols = slice(h * vdim, (h + 1) * vdim)
        one = jnp.dot(lat, vup_ref[:, cols], preferred_element_type=F32)
        squares = squares + jnp.sum(one * one, axis=1, keepdims=True)
        scaled = (one * gain_ref[:, cols]).astype(BF16)
        for t in range(tp):
            gated[t % 2, (t // 2) * share:(t // 2 + 1) * share, cols] = (
                scaled[t * share:(t + 1) * share])
        if h == 0:
            near(0, 2, 0)
            near(1, 1, 1)
        elif h == heads // 2:
            near(0, 2, 1)
    sq_out[...] = jnp.broadcast_to(squares, sq_out.shape)
    own[3].wait()

    tile = width // 4

    def project(which, put):
        def one(c, _):
            cols = pl.ds(pl.multiple_of(c * tile, tile), tile)
            got = jnp.dot(gated[which], ow[:, cols], preferred_element_type=F32)
            put(cols, got.reshape(nx, share, tile))
            return 0
        lax.fori_loop(0, 4, one, 0)

    def put_out(cols, got):
        pout[:, :, cols] = got.astype(BF16)

    def put_keep(cols, got):
        keep[:, :, cols] = got

    project(1 - core, put_out)
    remote(pout, pin, r_send.at[0], r_recv.at[0], (sp, pcore))
    for j in range(1, tp):
        to = lax.rem(me + j, tp)
        remote(sq_out.at[pl.ds(pl.multiple_of(to * share, share), share)], sq_in.at[j],
               s_send.at[j], s_recv.at[j], (sp, to))
    project(core, put_keep)
    arrived(pin, r_send.at[0], r_recv.at[0])
    for kx in range(1, nx):
        xi = flip(x, kx)
        xout[kx] = (keep[xi] + pin[xi].astype(F32)).astype(BF16)
        remote(xout.at[kx], xin.at[kx], r_send.at[kx], r_recv.at[kx], (sp, along(kx, core)))
    far(0, 1, 0, 1)
    near(1, 2, 0)
    far(1, 0, 0, 1)
    near(1, 2, 1)
    summed = keep[x] + pin[x].astype(F32)
    square = sq_out[pl.ds(pl.multiple_of(me * share, share), share)]
    for j in range(1, tp):
        arrived(sq_in.at[j], s_send.at[j], s_recv.at[j])
        square = square + sq_in[j]
    for kx in range(1, nx):
        arrived(xin.at[kx], r_send.at[kx], r_recv.at[kx])
        summed = summed + xin[kx].astype(F32)
    row_scale = lax.rsqrt(square[:, :1] / (heads * tp * vdim) + EPS)
    middle = stream_ref[...].astype(F32) + row_scale * summed
    mid[...] = middle
    norm = lax.rsqrt(jnp.mean(middle * middle, axis=1, keepdims=True) + EPS)

    def seat(kx, c):
        return c * nx + flip(x, kx)

    xs[0, seat(0, core)] = (middle * norm * ngain_ref[...]).astype(BF16)

    def hand(s, kx):
        ref = xs.at[s, seat(kx, core)]
        remote(ref, ref, g_send.at[1, s, kx], g_recv.at[1, s, kx], (sp, pcore))

    def spread(s):
        ref = xs.at[s, seat(0, core)]
        for kx in range(1, nx):
            remote(ref, ref, g_send.at[0, s, kx], g_recv.at[0, s, kx], (sp, along(kx, core)))
        hand(s, 0)

    def collect(s):
        for kx in range(1, nx):
            arrived(xs.at[s, seat(kx, core)], g_send.at[0, s, kx], g_recv.at[0, s, kx])
            hand(s, kx)

    def settled(s):
        for kx in range(nx):
            arrived(xs.at[s, seat(kx, 1 - core)], g_send.at[1, s, kx], g_recv.at[1, s, kx])

    ref = xs.at[0, seat(0, core)]
    remote(ref, xs.at[1, seat(0, core)], g_send.at[0, 0, 0], g_recv.at[0, 0, 0], (mate, me))
    spread(0)
    far(0, 2, 0, 1)
    near(0, m - 1, 0, 1)
    collect(0)
    settled(0)
    far(1, 1, 0)
    far(0, m - 1, 0, 1)

    wide = 512 if hh % 512 == 0 else 128

    def first(s):
        for c in range(hh // wide):
            cols = slice(c * wide, (c + 1) * wide)
            pre = jnp.dot(
                xs[s].reshape(rows, width), fi[:, cols], preferred_element_type=F32)
            pre = jnp.maximum(pre, 0.0)
            act[s, :, cols] = (pre * pre).astype(BF16)

    flow = []
    for k in range(m):
        flow.append((0, at(k)))
    for g in others:
        for ky in range(ny):
            flow.append((g, (1 - half) * m + (g - 1) * ny + flip(y, ky)))

    def stage_dot(i, u):
        got = jnp.dot(act[u], fo[flow[i][1]], preferred_element_type=F32)
        fresh[...] = got.reshape(2, nx, share, dblk)
        mixed[i, u] = fresh[core]
        mpo[i, u] = fresh[1 - core].astype(BF16)
        remote(mpo.at[i, u], mpi.at[i, u], mp_send.at[i, u], mp_recv.at[i, u], (sp, pcore))

    def stage_core(i, u):
        arrived(mpi.at[i, u], mp_send.at[i, u], mp_recv.at[i, u])
        for kx in range(1, nx):
            xi = flip(x, kx)
            mxo[i, u, kx] = (
                mixed[i, u, xi] + mpi[i, u, xi].astype(F32)).astype(BF16)
            remote(mxo.at[i, u, kx], mxi.at[i, u, kx], mx_send.at[i, u, kx],
                   mx_recv.at[i, u, kx], (sp, along(kx, core)))

    def stage_x(i, u):
        s = flow[i][1]
        v = mixed[i, u, x] + mpi[i, u, x].astype(F32)
        for kx in range(1, nx):
            arrived(mxi.at[i, u, kx], mx_send.at[i, u, kx], mx_recv.at[i, u, kx])
            v = v + mxi[i, u, kx].astype(F32)
        if u == 1:
            mzo[s] = v.astype(BF16)
            remote(mzo.at[s], mzi.at[s], mz_send.at[s], mz_recv.at[s], (mate, me))
        else:
            cols = pl.ds(pl.multiple_of(s * dblk, dblk), dblk)
            mid[:, cols] = mid[:, cols] + v

    to_core, to_x = [], []

    def drain(cores, xs_left):
        while len(to_core) > cores:
            stage_core(*to_core[0])
            to_x.append(to_core.pop(0))
        while len(to_x) > xs_left:
            stage_x(*to_x.pop(0))

    def push(i, u):
        stage_dot(i, u)
        to_core.append((i, u))
        drain(2, 4)

    arrived(xs.at[1, seat(0, core)], g_send.at[0, 0, 0], g_recv.at[0, 0, 0])
    spread(1)
    first(0)
    near(1, m - 1, 0, 1)
    for i in range(m):
        push(i, 0)
    drain(0, 8)
    far(1, 1, 1)
    collect(1)
    settled(1)
    first(1)
    far(1, 2, 1)
    for i in range(m):
        push(i, 1)
    far(1, 2, 0)
    far(1, m - 1, 0, 1)
    for i in range(m, n):
        push(i, 1)
    for i in range(m, n):
        push(i, 0)
    drain(0, 0)
    for i in range(n):
        s = flow[i][1]
        arrived(mzi.at[s], mz_send.at[s], mz_recv.at[s])
        cols = pl.ds(pl.multiple_of(s * dblk, dblk), dblk)
        out_ref[:, cols] = (mid[:, cols] + mzi[s].astype(F32)).astype(BF16)

    for cp in sends:
        cp.wait_send()
    for hm, cp in guarded:
        pl.when(is_inner(hm))(cp.wait_send)


def body(
    n, tp,
    stream, query_nope, query_rope, latent, rope_key, latent_gain,
    key_up, value_up, out_gain, out_weight, norm_gain, ff_in, ff_out,
):
    rows, heads = query_nope.shape[:2]
    width = stream.shape[1]
    latent_width = latent.shape[1]
    rope = rope_key.shape[1]
    pad = -rope % LANES
    dblk, hidden = ff_in.shape
    share = rows // tp
    positions = (lax.axis_index("sp") * rows + jnp.arange(rows, dtype=jnp.int32)).astype(F32)
    lat_full = latent.astype(F32)
    normed = (
        lat_full
        * lax.rsqrt(jnp.mean(lat_full * lat_full, axis=-1, keepdims=True) + EPS)
        * latent_gain
    ).astype(BF16)
    keys_rot = turn(rope_key, positions).astype(BF16)
    query_rot = turn(query_rope, positions).astype(BF16)
    query_lat = jnp.einsum(
        "thn,lhn->htl", query_nope, key_up, preferred_element_type=F32
    ).astype(BF16)
    kv = jnp.concatenate([normed, keys_rot, jnp.zeros((rows, pad), BF16)], axis=1)
    q = jnp.concatenate(
        [query_lat, query_rot.transpose(1, 0, 2), jnp.zeros((heads, rows, pad), BF16)], axis=2
    )
    keys = n * rows
    nz, ny = ring_shape(n)
    hz, m, nx = nz // 2, n // 2, tp // 2
    chunk = ny * rows
    hh = hidden // 2
    wide = kv.shape[1]
    vm = pl.BlockSpec(memory_space=pltpu.VMEM)
    hbm = pl.BlockSpec(memory_space=pl.ANY)
    dma = pltpu.SemaphoreType.DMA
    return pl.pallas_call(
        functools.partial(kernel, n, tp, heads, latent_width, width),
        out_shape=jax.ShapeDtypeStruct((share, width), BF16),
        in_specs=[hbm, vm, vm, vm, hbm, vm, vm, hbm, hbm],
        out_specs=vm,
        scratch_shapes=[
            pltpu.VMEM((keys, wide), BF16),
            pltpu.VMEM((width, hh), BF16),
            pltpu.VMEM((n, hh, dblk), BF16),
            pltpu.VMEM(out_weight.shape, BF16),
            pltpu.VMEM((nz, heads, rows, chunk), F32),
            pltpu.VMEM((heads, rows, LANES), F32),
            pltpu.VMEM((rows, latent_width), F32),
            pltpu.VMEM((2, nx * share, out_weight.shape[0]), BF16),
            pltpu.VMEM((nx, share, width), BF16),
            pltpu.VMEM((nx, share, width), BF16),
            pltpu.VMEM((nx, share, width), F32),
            pltpu.VMEM((nx, share, width), BF16),
            pltpu.VMEM((nx, share, width), BF16),
            pltpu.VMEM((rows, LANES), F32),
            pltpu.VMEM((tp, share, LANES), F32),
            pltpu.VMEM((share, width), F32),
            pltpu.VMEM((2, tp, share, width), BF16),
            pltpu.VMEM((2, rows, hh), BF16),
            pltpu.VMEM((2, nx, share, dblk), F32),
            pltpu.VMEM((n, 2, nx, share, dblk), F32),
            pltpu.VMEM((n, 2, nx, share, dblk), BF16),
            pltpu.VMEM((n, 2, nx, share, dblk), BF16),
            pltpu.VMEM((n, 2, nx, share, dblk), BF16),
            pltpu.VMEM((n, 2, nx, share, dblk), BF16),
            pltpu.VMEM((n, share, dblk), BF16),
            pltpu.VMEM((n, share, dblk), BF16),
            dma((4,)),
            dma((n,)), dma((n,)), dma((n, nx)), dma((n, nx)), dma((n, nx)), dma((n, nx)),
            dma((2,)), dma((2, hz)),
            dma((2, hz + 1, 2, m)), dma((2, hz + 1, 2, m)),
            dma((tp,)), dma((tp,)), dma((nx,)), dma((nx,)),
            dma((2, 2, nx)), dma((2, 2, nx)),
            dma((n, 2)), dma((n, 2)), dma((n, 2, nx)), dma((n, 2, nx)), dma((n,)), dma((n,)),
        ],
        compiler_params=pltpu.CompilerParams(
            collective_id=0, has_side_effects=True, vmem_limit_bytes=63 * 1024 * 1024
        ),
    )(
        kv, q, value_up.reshape(latent_width, -1), out_gain[None, :], out_weight,
        stream, norm_gain[None, :], ff_in, ff_out,
    )


def solution(mesh):
    placed = (
        P(("sp", "tp"), None),
        P("sp", "tp", None),
        P("sp", "tp", None),
        P("sp", None),
        P("sp", None),
        P(),
        P(None, "tp", None),
        P(None, "tp", None),
        P("tp"),
        P("tp", None),
        P(),
        P("sp", "tp"),
        P("tp", "sp"),
    )
    return jax.shard_map(
        functools.partial(body, mesh.shape["sp"], mesh.shape["tp"]),
        mesh=mesh, in_specs=placed, out_specs=P(("sp", "tp"), None), check_vma=False
    )
```

time: 204 us -> 157 us (0.77)
  Pallas kernels: 194 us -> 147 us
    pallas_call x1, Pallas kernels: 194 us -> 147 us  [body(): pl.pallas_call(functools.partial(kernel, n, tp, heads, latent_width, widt...]
where the time goes in v1:
time: 157 us
  Pallas kernels  147 us (94%)
  local copies, waits for them, and re-layouts  5.15 us (3%)
  other arithmetic  4.46 us (3%)
    pallas_call x1, Pallas kernels, body(): pl.pallas_call(functools.partial(kernel, n, tp, heads, latent_width, widt...  147 us
    unnamed x14, local copies, waits for them, and re-layouts  5.07 us

profile of v1, /device:TPU:0, one launch (start us, length us, event | category | flops | bytes accessed | tf_op | source)
XLA Modules:
  0.0 156.9 jit_solution(7432251531849555770)
XLA Ops:
  0.0 0.0 copy-start
  0.0 1.0 copy.18
  1.0 0.8 multiply_cosine_fusion
  1.9 1.2 copy.22
  3.0 0.1 convert_element_type.29
  3.1 0.0 copy-start.3
  3.1 0.4 subtract_convert_fusion
  3.5 0.2 maximum_bitcast_fusion
  3.7 0.1 pad.8.clone
  3.8 0.0 copy-done
  3.8 0.3 copy-done.3
  4.1 0.6 convolution_convert_fusion
  4.7 0.0 copy-start.1
  4.7 0.0 copy-start.4
  4.7 1.7 %maximum_maximum_fusion.q_ref = bf16[4,384,640]{2,1,0:T(8,128)(2,1)} fusion(bf16[4,384,64]{2,1,0:T(8,128)(2,1)S(1)} %maximum_bitcast_fusion, bf16[4,384,512]{2,1,0:T(8,128)(2,1)S(1)} %convolution_convert_fusion, bf16[640]{0:T(1024)(128)(2,1)S(1)} %pad.8.clone), kind=kLoop, calls=%fused_computation | loop fusion | flops 5898240 | bytes 3736832 | tf_op jit(solution)/shard_map/concatenate | solution.py:549
  6.4 0.0 copy-done.1
  6.4 0.2 fusion
  6.6 0.0 copy-done.4
  6.6 0.2 fusion.2
  6.7 0.9 maximum_maximum_fusion.1.kv_ref
  7.7 0.0 copy-done.2
  7.7 0.9 copy.29
  8.5 146.6 %shard_map.127 = bf16[96,2048]{1,0:T(8,128)(2,1)} custom-call(bf16[384,640]{1,0:T(8,128)(2,1)} %maximum_maximum_fusion.1.kv_ref, bf16[4,384,640]{2,1,0:T(8,128)(2,1)} %maximum_maximum_fusion.q_ref, bf16[512,512]{1,0:T(8,128)(2,1)} %bitcast.8, f32[1,512]{1,0:T(1,128)} %bitcast.11, bf16[512,2048]{1,0:T(8,128)(2,1)} %ow_ref.1, bf16[96,2048]{1,0:T(8,128)(2,1)} %stream_ref.1, ...), custom_call_target="tpu_custom_call" | custom-call | tf_op jit(solution)/shard_map/pallas_call | solution.py:561
  155.1 1.8 %copy.31 = bf16[96,2048]{1,0:T(8,128)(2,1)} copy(bf16[96,2048]{1,0:T(8,128)(2,1)} %shard_map.127) | data formatting | bytes 786432
  (6 shorter events, 0.0 us)
Async XLA Ops:
  0.0 3.8 %copy-start = (bf16[512,4,128]{2,1,0:T(4,128)(2,1)S(1)}, bf16[512,4,128]{2,1,0:T(4,128)(2,1)}, u32[]{:S(2)}) copy-start(bf16[512,4,128]{2,1,0:T(4,128)(2,1)} %param.19) | copy-start | bytes 1572868
  3.1 1.0 copy-start.3
  4.7 1.7 %copy-start.1 = (bf16[384,512]{1,0:T(8,128)(2,1)S(1)}, bf16[384,512]{1,0:T(8,128)(2,1)}, u32[]{:S(2)}) copy-start(bf16[384,512]{1,0:T(8,128)(2,1)} %param.16) | copy-start | bytes 1179652
  4.7 1.9 %copy-start.4 = (f32[512]{0:T(512)S(1)}, f32[512]{0:T(512)}, u32[]{:S(2)}) copy-start(f32[512]{0:T(512)} %param.18) | copy-start | bytes 6148
  6.4 1.3 copy-start.2

commit v2 on v1

--- a/solution.py
+++ b/solution.py
@@ -14,28 +14,6 @@
 BF16 = jnp.bfloat16
 MESH = pl.DeviceIdType.MESH
 LANES = 128
-
-
-def turn(values, positions):
-    full_width = values.shape[-1]
-    half_width = full_width // 2
-    inverse = jnp.power(THETA, -jnp.arange(0, full_width, 2, dtype=F32) / full_width)
-    angles = positions[:, None] * inverse[None, :]
-    cosine = jnp.cos(angles)
-    sine_part = jnp.sin(angles)
-    if values.ndim == 3:
-        cosine = cosine[:, None, :]
-        sine_part = sine_part[:, None, :]
-    vector = values.astype(F32)
-    lower_half = vector[..., :half_width]
-    upper_half = vector[..., half_width:]
-    return jnp.concatenate(
-        [
-            lower_half * cosine - upper_half * sine_part,
-            lower_half * sine_part + upper_half * cosine,
-        ],
-        axis=-1,
-    )
 
 
 def ring_shape(n):
@@ -77,9 +55,10 @@
 
 def kernel(
     n, tp, heads, latent_width, width,
-    kv_ref, q_ref, vup_ref, gain_ref, ow_ref, stream_ref, ngain_ref, ffin_ref, ffout_ref,
+    lat_ref, lgain_ref, rk_ref, cos_ref, sin_ref, qn_ref, qr_ref, kup_ref, vup_ref,
+    gain_ref, ow_ref, stream_ref, ngain_ref, ffin_ref, ffout_ref,
     out_ref,
-    kv, fi, fo, ow, sc, top, acc, gated, pout, pin, keep, xout, xin, sq_out, sq_in, mid, xs, act,
+    qraw, kraw, vraw, plain, q, vup, kv, fi, fo, ow, sc, top, acc, gated, pout, pin, keep, xout, xin, sq_out, sq_in, mid, xs, act,
     fresh, mixed, mpo, mpi, mxo, mxi, mzo, mzi,
     local_sem, ka_send, ka_recv, kx_send, kx_recv, kp_send, kp_recv,
     c_send, c_recv, w_send, w_recv,
@@ -96,7 +75,7 @@
     zl = lax.div(local, ny)
     mate = lax.rem(sp + m, n)
     pcore = me + 1 - 2 * core
-    rows = q_ref.shape[1]
+    rows = q.shape[1]
     share = rows // tp
     dblk = width // n
     hh = act.shape[2]
@@ -136,13 +115,33 @@
         return pl.ds(pl.multiple_of(s * dblk, dblk), dblk)
 
     own = [
-        pltpu.make_async_copy(kv_ref, kv.at[pl.ds(sp * rows, rows)], local_sem.at[0]),
+        pltpu.make_async_copy(qn_ref, qraw, local_sem.at[0]),
         pltpu.make_async_copy(ffin_ref.at[:, lanes(half)], fi.at[block_rows(sp)], local_sem.at[1]),
         pltpu.make_async_copy(ffout_ref.at[deep(half)], fo.at[sp], local_sem.at[2]),
         pltpu.make_async_copy(ow_ref, ow, local_sem.at[3]),
+        pltpu.make_async_copy(kup_ref, kraw, local_sem.at[4]),
+        pltpu.make_async_copy(vup_ref, vraw, local_sem.at[5]),
     ]
-    for cp in own:
-        cp.start()
+    for c in (1, 2, 0, 4, 5, 3):
+        own[c].start()
+
+    rope = rk_ref.shape[0]
+    hw = rope // 2
+
+    def turned(values):
+        v = values.astype(F32)
+        a, b = v[:hw], v[hw:]
+        c, s = cos_ref[...], sin_ref[...]
+        parts = [a * c - b * s, a * s + b * c]
+        if rope % LANES:
+            parts.append(jnp.zeros((-rope % LANES, rows), F32))
+        return jnp.concatenate(parts, axis=0).T.astype(BF16)
+
+    here = pl.ds(pl.multiple_of(sp * rows, rows), rows)
+    full = lat_ref[...].astype(F32)
+    spread_out = lax.rsqrt(jnp.mean(full * full, axis=-1, keepdims=True) + EPS)
+    kv[here, pl.ds(0, latent_width)] = (full * spread_out * lgain_ref[...]).astype(BF16)
+    kv[here, pl.ds(latent_width, kv.shape[1] - latent_width)] = turned(rk_ref[...])
 
     barrier = pltpu.get_barrier_semaphore()
     for i in range(1, n):
@@ -215,9 +214,10 @@
         hm = home(way, step)
         s = source(g, hm)
         ref = w_ref(b, s, way)
-        cp = pltpu.make_async_remote_copy(
-            ref, ref, w_send.at[b, g, way, step], w_recv.at[b, g, way, step],
-            device_id=(at(1 - 2 * way), me), device_id_type=MESH)
+        if step < m - 1:
+            cp = pltpu.make_async_remote_copy(
+                ref, ref, w_send.at[b, g, way, step], w_recv.at[b, g, way, step],
+                device_id=(at(1 - 2 * way), me), device_id_type=MESH)
 
         def go():
             if step > 0:
@@ -255,7 +255,6 @@
             for g in others:
                 do(b, g, step, k)
 
-    own[0].wait()
     mine = piece(sp, me)
     for ky in range(1, ny):
         remote(mine, mine, ka_send.at[ky], ka_recv.at[ky], (space(0, ky), me))
@@ -264,14 +263,14 @@
     own[1].wait()
     near(0, 0, 0, 1)
 
-    scale = 1.0 / math.sqrt(LANES + (q_ref.shape[2] - latent_width) // 2)
+    scale = 1.0 / math.sqrt(LANES + rope)
 
     def score(kz):
         keys = pl.ds(pl.multiple_of(flip(z, kz) * chunk, chunk), chunk)
 
         def one(h, _):
             s = lax.dot_general(
-                q_ref[h], kv[keys, :], (((1,), (1,)), ((), ())),
+                q[h], kv[keys, :], (((1,), (1,)), ((), ())),
                 preferred_element_type=F32) * scale
             sc[kz, h] = s
             best = jnp.max(s, axis=1, keepdims=True)
@@ -282,9 +281,31 @@
 
         lax.fori_loop(0, heads, one, 0)
 
+    def unpack(raw, count):
+        plain[pl.ds(0, count * heads), :] = raw[...].astype(F32)
+
+    def head_rows(h, count):
+        return plain[pl.ds(h, count, stride=heads), :].astype(BF16)
+
+    own[0].wait()
+    unpack(qraw, rows)
+    for h in range(heads):
+        q[h, :, pl.ds(0, vdim)] = head_rows(h, rows)
+    own[4].wait()
+    unpack(kraw, latent_width)
+    for h in range(heads):
+        q[h, :, pl.ds(0, latent_width)] = lax.dot_general(
+            q[h, :, pl.ds(0, vdim)], head_rows(h, latent_width), (((1,), (1,)), ((), ())),
+            preferred_element_type=F32).astype(BF16)
     for ky in range(1, ny):
         arrive(0, ky)
     arrive(1, 0)
+    for h in range(heads):
+        q[h, :, pl.ds(latent_width, q.shape[2] - latent_width)] = turned(qr_ref[h])
+    own[5].wait()
+    unpack(vraw, latent_width)
+    for h in range(heads):
+        vup[:, h * vdim:(h + 1) * vdim] = head_rows(h, latent_width)
     for ky in range(1, ny):
         across(0, ky)
     for kz in range(2, nz):
@@ -335,7 +356,7 @@
         den = lax.fori_loop(0, nz, gather, jnp.zeros((rows, 1), F32))
         lat = (acc[...] / den).astype(BF16)
         cols = slice(h * vdim, (h + 1) * vdim)
-        one = jnp.dot(lat, vup_ref[:, cols], preferred_element_type=F32)
+        one = jnp.dot(lat, vup[:, cols], preferred_element_type=F32)
         squares = squares + jnp.sum(one * one, axis=1, keepdims=True)
         scaled = (one * gain_ref[:, cols]).astype(BF16)
         for t in range(tp):
@@ -375,10 +396,9 @@
     arrived(pin, r_send.at[0], r_recv.at[0])
     for kx in range(1, nx):
         xi = flip(x, kx)
-        xout[kx] = (keep[xi] + pin[xi].astype(F32)).astype(BF16)
-        remote(xout.at[kx], xin.at[kx], r_send.at[kx], r_recv.at[kx], (sp, along(kx, core)))
+        xout[kx - 1] = (keep[xi] + pin[xi].astype(F32)).astype(BF16)
+        remote(xout.at[kx - 1], xin.at[kx - 1], r_send.at[kx], r_recv.at[kx], (sp, along(kx, core)))
     far(0, 1, 0, 1)
-    near(1, 2, 0)
     far(1, 0, 0, 1)
     near(1, 2, 1)
     summed = keep[x] + pin[x].astype(F32)
@@ -387,8 +407,8 @@
         arrived(sq_in.at[j], s_send.at[j], s_recv.at[j])
         square = square + sq_in[j]
     for kx in range(1, nx):
-        arrived(xin.at[kx], r_send.at[kx], r_recv.at[kx])
-        summed = summed + xin[kx].astype(F32)
+        arrived(xin.at[kx - 1], r_send.at[kx], r_recv.at[kx])
+        summed = summed + xin[kx - 1].astype(F32)
     row_scale = lax.rsqrt(square[:, :1] / (heads * tp * vdim) + EPS)
     middle = stream_ref[...].astype(F32) + row_scale * summed
     mid[...] = middle
@@ -426,6 +446,7 @@
     collect(0)
     settled(0)
     far(1, 1, 0)
+    near(1, 2, 0)
     far(0, m - 1, 0, 1)
 
     wide = 512 if hh % 512 == 0 else 128
@@ -456,17 +477,17 @@
         arrived(mpi.at[i, u], mp_send.at[i, u], mp_recv.at[i, u])
         for kx in range(1, nx):
             xi = flip(x, kx)
-            mxo[i, u, kx] = (
+            mxo[i, u, kx - 1] = (
                 mixed[i, u, xi] + mpi[i, u, xi].astype(F32)).astype(BF16)
-            remote(mxo.at[i, u, kx], mxi.at[i, u, kx], mx_send.at[i, u, kx],
+            remote(mxo.at[i, u, kx - 1], mxi.at[i, u, kx - 1], mx_send.at[i, u, kx],
                    mx_recv.at[i, u, kx], (sp, along(kx, core)))
 
     def stage_x(i, u):
         s = flow[i][1]
         v = mixed[i, u, x] + mpi[i, u, x].astype(F32)
         for kx in range(1, nx):
-            arrived(mxi.at[i, u, kx], mx_send.at[i, u, kx], mx_recv.at[i, u, kx])
-            v = v + mxi[i, u, kx].astype(F32)
+            arrived(mxi.at[i, u, kx - 1], mx_send.at[i, u, kx], mx_recv.at[i, u, kx])
+            v = v + mxi[i, u, kx - 1].astype(F32)
         if u == 1:
             mzo[s] = v.astype(BF16)
             remote(mzo.at[s], mzi.at[s], mz_send.at[s], mz_recv.at[s], (mate, me))
@@ -490,24 +511,31 @@
 
     arrived(xs.at[1, seat(0, core)], g_send.at[0, 0, 0], g_recv.at[0, 0, 0])
     spread(1)
+    far(1, 1, 1)
     first(0)
-    near(1, m - 1, 0, 1)
-    for i in range(m):
+    early = [0, 2] if m == 4 else [0]
+    late = [i for i in range(m) if i not in early]
+    for i in early:
         push(i, 0)
     drain(0, 8)
-    far(1, 1, 1)
     collect(1)
+    far(1, 2, 0)
+    far(1, 2, 1)
     settled(1)
     first(1)
-    far(1, 2, 1)
-    for i in range(m):
+    for i in early:
         push(i, 1)
-    far(1, 2, 0)
-    far(1, m - 1, 0, 1)
-    for i in range(m, n):
-        push(i, 1)
-    for i in range(m, n):
-        push(i, 0)
+    near(1, m - 1, 0, 1)
+    for u in (1, 0):
+        for i in late:
+            push(i, u)
+    for g in others:
+        for k in range(2):
+            do(1, g, m - 1, k)
+        for u in (1, 0):
+            for i in range(m, n):
+                if flow[i][0] == g:
+                    push(i, u)
     drain(0, 0)
     for i in range(n):
         s = flow[i][1]
@@ -530,40 +558,32 @@
     width = stream.shape[1]
     latent_width = latent.shape[1]
     rope = rope_key.shape[1]
-    pad = -rope % LANES
     dblk, hidden = ff_in.shape
     share = rows // tp
     positions = (lax.axis_index("sp") * rows + jnp.arange(rows, dtype=jnp.int32)).astype(F32)
-    lat_full = latent.astype(F32)
-    normed = (
-        lat_full
-        * lax.rsqrt(jnp.mean(lat_full * lat_full, axis=-1, keepdims=True) + EPS)
-        * latent_gain
-    ).astype(BF16)
-    keys_rot = turn(rope_key, positions).astype(BF16)
-    query_rot = turn(query_rope, positions).astype(BF16)
-    query_lat = jnp.einsum(
-        "thn,lhn->htl", query_nope, key_up, preferred_element_type=F32
-    ).astype(BF16)
-    kv = jnp.concatenate([normed, keys_rot, jnp.zeros((rows, pad), BF16)], axis=1)
-    q = jnp.concatenate(
-        [query_lat, query_rot.transpose(1, 0, 2), jnp.zeros((heads, rows, pad), BF16)], axis=2
-    )
+    inverse = jnp.power(THETA, -jnp.arange(0, rope, 2, dtype=F32) / rope)
+    angles = positions[None, :] * inverse[:, None]
+    wide = latent_width + rope + (-rope) % LANES
     keys = n * rows
     nz, ny = ring_shape(n)
     hz, m, nx = nz // 2, n // 2, tp // 2
     chunk = ny * rows
     hh = hidden // 2
-    wide = kv.shape[1]
     vm = pl.BlockSpec(memory_space=pltpu.VMEM)
     hbm = pl.BlockSpec(memory_space=pl.ANY)
     dma = pltpu.SemaphoreType.DMA
     return pl.pallas_call(
         functools.partial(kernel, n, tp, heads, latent_width, width),
         out_shape=jax.ShapeDtypeStruct((share, width), BF16),
-        in_specs=[hbm, vm, vm, vm, hbm, vm, vm, hbm, hbm],
+        in_specs=[vm, vm, vm, vm, vm, hbm, vm, hbm, hbm, vm, hbm, vm, vm, hbm, hbm],
         out_specs=vm,
         scratch_shapes=[
+            pltpu.VMEM((rows * heads, LANES), BF16),
+            pltpu.VMEM((latent_width * heads, LANES), BF16),
+            pltpu.VMEM((latent_width * heads, LANES), BF16),
+            pltpu.VMEM((max(rows, latent_width) * heads, LANES), F32),
+            pltpu.VMEM((heads, rows, wide), BF16),
+            pltpu.VMEM((latent_width, heads * LANES), BF16),
             pltpu.VMEM((keys, wide), BF16),
             pltpu.VMEM((width, hh), BF16),
             pltpu.VMEM((n, hh, dblk), BF16),
@@ -575,8 +595,8 @@
             pltpu.VMEM((nx, share, width), BF16),
             pltpu.VMEM((nx, share, width), BF16),
             pltpu.VMEM((nx, share, width), F32),
-            pltpu.VMEM((nx, share, width), BF16),
-            pltpu.VMEM((nx, share, width), BF16),
+            pltpu.VMEM((max(nx - 1, 1), share, width), BF16),
+            pltpu.VMEM((max(nx - 1, 1), share, width), BF16),
             pltpu.VMEM((rows, LANES), F32),
             pltpu.VMEM((tp, share, LANES), F32),
             pltpu.VMEM((share, width), F32),
@@ -586,11 +606,11 @@
             pltpu.VMEM((n, 2, nx, share, dblk), F32),
             pltpu.VMEM((n, 2, nx, share, dblk), BF16),
             pltpu.VMEM((n, 2, nx, share, dblk), BF16),
-            pltpu.VMEM((n, 2, nx, share, dblk), BF16),
-            pltpu.VMEM((n, 2, nx, share, dblk), BF16),
+            pltpu.VMEM((n, 2, max(nx - 1, 1), share, dblk), BF16),
+            pltpu.VMEM((n, 2, max(nx - 1, 1), share, dblk), BF16),
             pltpu.VMEM((n, share, dblk), BF16),
             pltpu.VMEM((n, share, dblk), BF16),
-            dma((4,)),
+            dma((6,)),
             dma((n,)), dma((n,)), dma((n, nx)), dma((n, nx)), dma((n, nx)), dma((n, nx)),
             dma((2,)), dma((2, hz)),
             dma((2, hz + 1, 2, m)), dma((2, hz + 1, 2, m)),
@@ -602,7 +622,9 @@
             collective_id=0, has_side_effects=True, vmem_limit_bytes=63 * 1024 * 1024
         ),
     )(
-        kv, q, value_up.reshape(latent_width, -1), out_gain[None, :], out_weight,
+        latent, latent_gain[None, :], rope_key.T, jnp.cos(angles), jnp.sin(angles),
+        query_nope.reshape(-1, LANES), query_rope.transpose(1, 2, 0),
+        key_up.reshape(-1, LANES), value_up.reshape(-1, LANES), out_gain[None, :], out_weight,
         stream, norm_gain[None, :], ff_in, ff_out,
     )
 

time: 157 us -> 138 us (0.88)
  Pallas kernels: 147 us -> 135 us
  other arithmetic: 4.46 us -> 0.92 us
  local copies, waits for them, and re-layouts: 5.15 us -> 1.77 us
    pallas_call x1, Pallas kernels: 147 us -> 135 us  [body(): pl.pallas_call(functools.partial(kernel, n, tp, heads, latent_width, widt...]
    unnamed x14 -> x1, local copies, waits for them, and re-layouts: 5.07 us -> 1.77 us
    concatenate x2 -> x0, other arithmetic: 2.63 us -> none  [the longest x1 1.69 us: body(): jnp.concatenate([query_lat, query_rot.transpose(1, 0, 2), jnp.zeros((head...]
where the time goes in v2:
time: 138 us
  Pallas kernels  135 us (98%)
  local copies, waits for them, and re-layouts  1.77 us (1%)
    pallas_call x1, Pallas kernels, body(): pl.pallas_call(functools.partial(kernel, n, tp, heads, latent_width, widt...  135 us

profile of v2, /device:TPU:0, one launch (start us, length us, event | category | flops | bytes accessed | tf_op | source)
XLA Modules:
  0.0 137.8 jit_solution(10867436498149210882)
XLA Ops:
  0.0 0.9 multiply_sine_fusion
  0.9 135.1 %shard_map.127 = bf16[96,2048]{1,0:T(8,128)(2,1)} custom-call(bf16[384,512]{1,0:T(8,128)(2,1)} %lat_ref.1, f32[1,512]{1,0:T(1,128)} %bitcast.14, bf16[64,384]{1,0:T(8,128)(2,1)} %bitcast.12, f32[32,384]{1,0:T(8,128)} %get-tuple-element.6.cos_ref, f32[32,384]{1,0:T(8,128)} %get-tuple-element.5.sin_ref, bf16[1536,128]{1,0:T(8,128)(2,1)} %bitcast.10, ...), custom_call_target="tpu_custom_call" | custom-call | tf_op jit(solution)/shard_map/pallas_call | solution.py:575
  136.0 1.8 %copy.15 = bf16[96,2048]{1,0:T(8,128)(2,1)} copy(bf16[96,2048]{1,0:T(8,128)(2,1)} %shard_map.127) | data formatting | bytes 786432
  (2 shorter events, 0.0 us)

commit v3 on v2

--- a/solution.py
+++ b/solution.py
@@ -58,7 +58,7 @@
     lat_ref, lgain_ref, rk_ref, cos_ref, sin_ref, qn_ref, qr_ref, kup_ref, vup_ref,
     gain_ref, ow_ref, stream_ref, ngain_ref, ffin_ref, ffout_ref,
     out_ref,
-    qraw, kraw, vraw, plain, q, vup, kv, fi, fo, ow, sc, top, acc, gated, pout, pin, keep, xout, xin, sq_out, sq_in, mid, xs, act,
+    qraw, kraw, vraw, plain, rope_q, base, q, vup, kv, fi, fo, ow, sc, top, acc, gated, pout, pin, keep, xout, xin, sq_out, sq_in, mid, xs, act,
     fresh, mixed, mpo, mpi, mxo, mxi, mzo, mzi,
     local_sem, ka_send, ka_recv, kx_send, kx_recv, kp_send, kp_recv,
     c_send, c_recv, w_send, w_recv,
@@ -79,7 +79,7 @@
     share = rows // tp
     dblk = width // n
     hh = act.shape[2]
-    chunk = sc.shape[3]
+    chunk = sc.shape[2]
     vdim = LANES
     pos = ring_pos(hz, ny, local)
 
@@ -114,6 +114,13 @@
     def block_rows(s):
         return pl.ds(pl.multiple_of(s * dblk, dblk), dblk)
 
+    barrier = pltpu.get_barrier_semaphore()
+    for i in range(1, n):
+        pl.semaphore_signal(
+            barrier, inc=1, device_id=(lax.rem(sp + i, n), me), device_id_type=MESH)
+    for j in range(1, tp):
+        pl.semaphore_signal(
+            barrier, inc=1, device_id=(sp, lax.rem(me + j, tp)), device_id_type=MESH)
     own = [
         pltpu.make_async_copy(qn_ref, qraw, local_sem.at[0]),
         pltpu.make_async_copy(ffin_ref.at[:, lanes(half)], fi.at[block_rows(sp)], local_sem.at[1]),
@@ -121,8 +128,10 @@
         pltpu.make_async_copy(ow_ref, ow, local_sem.at[3]),
         pltpu.make_async_copy(kup_ref, kraw, local_sem.at[4]),
         pltpu.make_async_copy(vup_ref, vraw, local_sem.at[5]),
+        pltpu.make_async_copy(qr_ref, rope_q, local_sem.at[6]),
+        pltpu.make_async_copy(stream_ref, base, local_sem.at[7]),
     ]
-    for c in (1, 2, 0, 4, 5, 3):
+    for c in (1, 2, 0, 4, 6, 5, 3, 7):
         own[c].start()
 
     rope = rk_ref.shape[0]
@@ -143,13 +152,6 @@
     kv[here, pl.ds(0, latent_width)] = (full * spread_out * lgain_ref[...]).astype(BF16)
     kv[here, pl.ds(latent_width, kv.shape[1] - latent_width)] = turned(rk_ref[...])
 
-    barrier = pltpu.get_barrier_semaphore()
-    for i in range(1, n):
-        pl.semaphore_signal(
-            barrier, inc=1, device_id=(lax.rem(sp + i, n), me), device_id_type=MESH)
-    for j in range(1, tp):
-        pl.semaphore_signal(
-            barrier, inc=1, device_id=(sp, lax.rem(me + j, tp)), device_id_type=MESH)
     pl.semaphore_wait(barrier, n + tp - 2)
 
     def piece(s, t):
@@ -250,9 +252,9 @@
         for k in ks:
             do(b, 0, step, k)
 
-    def far(b, step, *ks):
-        for k in ks:
-            for g in others:
+    def far(b, step, *ks, groups=None):
+        for g in groups or others:
+            for k in ks:
                 do(b, g, step, k)
 
     mine = piece(sp, me)
@@ -263,23 +265,26 @@
     own[1].wait()
     near(0, 0, 0, 1)
 
-    scale = 1.0 / math.sqrt(LANES + rope)
+    scale = math.log2(math.e) / math.sqrt(LANES + rope)
+    strip = 2 * LANES
+    team = heads * rows
 
     def score(kz):
-        keys = pl.ds(pl.multiple_of(flip(z, kz) * chunk, chunk), chunk)
-
-        def one(h, _):
+        base = flip(z, kz) * chunk
+
+        def one(t, _):
+            keys = pl.ds(pl.multiple_of(base + t * strip, strip), strip)
             s = lax.dot_general(
-                q[h], kv[keys, :], (((1,), (1,)), ((), ())),
+                q[...].reshape(team, q.shape[2]), kv[keys, :], (((1,), (1,)), ((), ())),
                 preferred_element_type=F32) * scale
-            sc[kz, h] = s
-            best = jnp.max(s, axis=1, keepdims=True)
-            if kz > 0:
-                best = jnp.maximum(best, top[h][:, :1])
-            top[h] = jnp.broadcast_to(best, (rows, LANES))
+            sc[kz, :, pl.ds(pl.multiple_of(t * strip, strip), strip)] = s
+            best = jnp.maximum(s[:, :LANES], s[:, LANES:])
+            top[...] = jnp.maximum(top[...], best)
             return 0
 
-        lax.fori_loop(0, heads, one, 0)
+        lax.fori_loop(0, chunk // strip, one, 0)
+
+    top[...] = jnp.full(top.shape, -jnp.inf, F32)
 
     def unpack(raw, count):
         plain[pl.ds(0, count * heads), :] = raw[...].astype(F32)
@@ -300,8 +305,9 @@
     for ky in range(1, ny):
         arrive(0, ky)
     arrive(1, 0)
+    own[6].wait()
     for h in range(heads):
-        q[h, :, pl.ds(latent_width, q.shape[2] - latent_width)] = turned(qr_ref[h])
+        q[h, :, pl.ds(latent_width, q.shape[2] - latent_width)] = turned(rope_q[h])
     own[5].wait()
     unpack(vraw, latent_width)
     for h in range(heads):
@@ -334,11 +340,12 @@
             near(1, 1, 0)
             near(0, 1, 1)
         elif kz == nz - 1:
-            far(0, 0, 0, 1)
+            near(0, 2, 0)
 
     squares = jnp.zeros((rows, 1), F32)
     for h in range(heads):
-        peak = top[h][:, :1]
+        team_rows = slice(h * rows, (h + 1) * rows)
+        peak = jnp.max(top[team_rows], axis=1, keepdims=True)
         acc[...] = jnp.zeros_like(acc)
 
         def gather(kz, den):
@@ -346,7 +353,7 @@
             zk = jnp.where(kz == 0, z, zk)
             for k in range(1, nz):
                 zk = jnp.where(kz == k, flip(z, k), zk)
-            e = jnp.exp(sc[kz, h] - peak)
+            e = jnp.exp2(sc[kz, team_rows] - peak)
             acc[...] += jnp.dot(
                 e.astype(BF16),
                 kv[pl.ds(pl.multiple_of(zk * chunk, chunk), chunk), pl.ds(0, latent_width)],
@@ -363,9 +370,10 @@
             gated[t % 2, (t // 2) * share:(t // 2 + 1) * share, cols] = (
                 scaled[t * share:(t + 1) * share])
         if h == 0:
-            near(0, 2, 0)
             near(1, 1, 1)
-        elif h == heads // 2:
+        if h == heads // 2 - 1:
+            far(0, 0, 0, 1)
+        if h == heads // 2:
             near(0, 2, 1)
     sq_out[...] = jnp.broadcast_to(squares, sq_out.shape)
     own[3].wait()
@@ -410,7 +418,8 @@
         arrived(xin.at[kx - 1], r_send.at[kx], r_recv.at[kx])
         summed = summed + xin[kx - 1].astype(F32)
     row_scale = lax.rsqrt(square[:, :1] / (heads * tp * vdim) + EPS)
-    middle = stream_ref[...].astype(F32) + row_scale * summed
+    own[7].wait()
+    middle = base[...].astype(F32) + row_scale * summed
     mid[...] = middle
     norm = lax.rsqrt(jnp.mean(middle * middle, axis=1, keepdims=True) + EPS)
 
@@ -511,25 +520,27 @@
 
     arrived(xs.at[1, seat(0, core)], g_send.at[0, 0, 0], g_recv.at[0, 0, 0])
     spread(1)
+    far(1, 1, 1, groups=others[:1])
+    first(0)
     far(1, 1, 1)
-    first(0)
     early = [0, 2] if m == 4 else [0]
     late = [i for i in range(m) if i not in early]
     for i in early:
         push(i, 0)
     drain(0, 8)
     collect(1)
-    far(1, 2, 0)
-    far(1, 2, 1)
+    far(1, 2, 0, 1, groups=others[:1])
     settled(1)
     first(1)
     for i in early:
         push(i, 1)
-    near(1, m - 1, 0, 1)
-    for u in (1, 0):
-        for i in late:
-            push(i, u)
+    far(1, 2, 0, 1)
     for g in others:
+        if g == 2:
+            near(1, m - 1, 0, 1)
+            for u in (1, 0):
+                for i in late:
+                    push(i, u)
         for k in range(2):
             do(1, g, m - 1, k)
         for u in (1, 0):
@@ -575,21 +586,23 @@
     return pl.pallas_call(
         functools.partial(kernel, n, tp, heads, latent_width, width),
         out_shape=jax.ShapeDtypeStruct((share, width), BF16),
-        in_specs=[vm, vm, vm, vm, vm, hbm, vm, hbm, hbm, vm, hbm, vm, vm, hbm, hbm],
+        in_specs=[vm, vm, vm, vm, vm, hbm, hbm, hbm, hbm, vm, hbm, hbm, vm, hbm, hbm],
         out_specs=vm,
         scratch_shapes=[
             pltpu.VMEM((rows * heads, LANES), BF16),
             pltpu.VMEM((latent_width * heads, LANES), BF16),
             pltpu.VMEM((latent_width * heads, LANES), BF16),
             pltpu.VMEM((max(rows, latent_width) * heads, LANES), F32),
+            pltpu.VMEM((heads, rope, rows), BF16),
+            pltpu.VMEM((share, width), BF16),
             pltpu.VMEM((heads, rows, wide), BF16),
             pltpu.VMEM((latent_width, heads * LANES), BF16),
             pltpu.VMEM((keys, wide), BF16),
             pltpu.VMEM((width, hh), BF16),
             pltpu.VMEM((n, hh, dblk), BF16),
             pltpu.VMEM(out_weight.shape, BF16),
-            pltpu.VMEM((nz, heads, rows, chunk), F32),
-            pltpu.VMEM((heads, rows, LANES), F32),
+            pltpu.VMEM((nz, heads * rows, chunk), F32),
+            pltpu.VMEM((heads * rows, LANES), F32),
             pltpu.VMEM((rows, latent_width), F32),
             pltpu.VMEM((2, nx * share, out_weight.shape[0]), BF16),
             pltpu.VMEM((nx, share, width), BF16),
@@ -610,7 +623,7 @@
             pltpu.VMEM((n, 2, max(nx - 1, 1), share, dblk), BF16),
             pltpu.VMEM((n, share, dblk), BF16),
             pltpu.VMEM((n, share, dblk), BF16),
-            dma((6,)),
+            dma((8,)),
             dma((n,)), dma((n,)), dma((n, nx)), dma((n, nx)), dma((n, nx)), dma((n, nx)),
             dma((2,)), dma((2, hz)),
             dma((2, hz + 1, 2, m)), dma((2, hz + 1, 2, m)),

time: 138 us -> 131 us (0.949)
  Pallas kernels: 135 us -> 128 us
    pallas_call x1, Pallas kernels: 135 us -> 128 us  [body(): pl.pallas_call(functools.partial(kernel, n, tp, heads, latent_width, widt...]
where the time goes in v3:
time: 131 us
  Pallas kernels  128 us (98%)
  local copies, waits for them, and re-layouts  1.77 us (1%)
    pallas_call x1, Pallas kernels, body(): pl.pallas_call(functools.partial(kernel, n, tp, heads, latent_width, widt...  128 us

profile of v3, /device:TPU:0, one launch (start us, length us, event | category | flops | bytes accessed | tf_op | source)
XLA Modules:
  0.0 131.0 jit_solution(15841451039475620985)
XLA Ops:
  0.0 0.9 multiply_sine_fusion
  0.9 128.3 %shard_map.127 = bf16[96,2048]{1,0:T(8,128)(2,1)} custom-call(bf16[384,512]{1,0:T(8,128)(2,1)} %lat_ref.1, f32[1,512]{1,0:T(1,128)} %bitcast.14, bf16[64,384]{1,0:T(8,128)(2,1)} %bitcast.12, f32[32,384]{1,0:T(8,128)} %get-tuple-element.6.cos_ref, f32[32,384]{1,0:T(8,128)} %get-tuple-element.5.sin_ref, bf16[1536,128]{1,0:T(8,128)(2,1)} %bitcast.10, ...), custom_call_target="tpu_custom_call" | custom-call | tf_op jit(solution)/shard_map/pallas_call | solution.py:586
  129.2 1.8 %copy.15 = bf16[96,2048]{1,0:T(8,128)(2,1)} copy(bf16[96,2048]{1,0:T(8,128)(2,1)} %shard_map.127) | data formatting | bytes 786432
  (2 shorter events, 0.0 us)

commit v4 on v3

--- a/solution.py
+++ b/solution.py
@@ -407,7 +407,6 @@
         xout[kx - 1] = (keep[xi] + pin[xi].astype(F32)).astype(BF16)
         remote(xout.at[kx - 1], xin.at[kx - 1], r_send.at[kx], r_recv.at[kx], (sp, along(kx, core)))
     far(0, 1, 0, 1)
-    far(1, 0, 0, 1)
     near(1, 2, 1)
     summed = keep[x] + pin[x].astype(F32)
     square = sq_out[pl.ds(pl.multiple_of(me * share, share), share)]
@@ -450,6 +449,7 @@
     ref = xs.at[0, seat(0, core)]
     remote(ref, xs.at[1, seat(0, core)], g_send.at[0, 0, 0], g_recv.at[0, 0, 0], (mate, me))
     spread(0)
+    far(1, 0, 0, 1)
     far(0, 2, 0, 1)
     near(0, m - 1, 0, 1)
     collect(0)
@@ -516,7 +516,7 @@
     def push(i, u):
         stage_dot(i, u)
         to_core.append((i, u))
-        drain(2, 4)
+        drain(1, 3)
 
     arrived(xs.at[1, seat(0, core)], g_send.at[0, 0, 0], g_recv.at[0, 0, 0])
     spread(1)
@@ -535,18 +535,24 @@
     for i in early:
         push(i, 1)
     far(1, 2, 0, 1)
+    rest = list(late)
     for g in others:
-        if g == 2:
-            near(1, m - 1, 0, 1)
-            for u in (1, 0):
-                for i in late:
-                    push(i, u)
+        mine_g = [i for i in range(m, n) if flow[i][0] == g]
         for k in range(2):
             do(1, g, m - 1, k)
-        for u in (1, 0):
-            for i in range(m, n):
-                if flow[i][0] == g:
-                    push(i, u)
+        for i in mine_g:
+            push(i, 1)
+        if g == 1:
+            near(1, m - 1, 0, 1)
+            for i in late:
+                push(i, 1)
+            for i in mine_g[:ny]:
+                push(i, 0)
+            rest += mine_g[ny:]
+        else:
+            rest += mine_g
+    for i in rest:
+        push(i, 0)
     drain(0, 0)
     for i in range(n):
         s = flow[i][1]

time: 131 us -> 131 us (level)
  no operation moved by 1% of the time
where the time goes in v4:
time: 131 us; the launch traced here: 130 us
  Pallas kernels  128 us (98%)
  local copies, waits for them, and re-layouts  1.77 us (1%)
    pallas_call x1, Pallas kernels, body(): pl.pallas_call(functools.partial(kernel, n, tp, heads, latent_width, widt...  128 us

profile of v4, /device:TPU:0, one launch (start us, length us, event | category | flops | bytes accessed | tf_op | source)
XLA Modules:
  0.0 130.5 jit_solution(15441458920919457353)
XLA Ops:
  0.0 0.9 multiply_sine_fusion
  0.9 127.8 %shard_map.127 = bf16[96,2048]{1,0:T(8,128)(2,1)} custom-call(bf16[384,512]{1,0:T(8,128)(2,1)} %lat_ref.1, f32[1,512]{1,0:T(1,128)} %bitcast.14, bf16[64,384]{1,0:T(8,128)(2,1)} %bitcast.12, f32[32,384]{1,0:T(8,128)} %get-tuple-element.6.cos_ref, f32[32,384]{1,0:T(8,128)} %get-tuple-element.5.sin_ref, bf16[1536,128]{1,0:T(8,128)(2,1)} %bitcast.10, ...), custom_call_target="tpu_custom_call" | custom-call | tf_op jit(solution)/shard_map/pallas_call | solution.py:592
  128.7 1.8 %copy.15 = bf16[96,2048]{1,0:T(8,128)(2,1)} copy(bf16[96,2048]{1,0:T(8,128)(2,1)} %shard_map.127) | data formatting | bytes 786432
  (2 shorter events, 0.0 us)

commit v5 on v4

--- a/solution.py
+++ b/solution.py
@@ -546,11 +546,7 @@
             near(1, m - 1, 0, 1)
             for i in late:
                 push(i, 1)
-            for i in mine_g[:ny]:
-                push(i, 0)
-            rest += mine_g[ny:]
-        else:
-            rest += mine_g
+        rest += mine_g
     for i in rest:
         push(i, 0)
     drain(0, 0)

time: 131 us -> 131 us (level)
  no operation moved by 1% of the time
where the time goes in v5:
time: 131 us; the launch traced here: 130 us
  Pallas kernels  128 us (98%)
  local copies, waits for them, and re-layouts  1.77 us (1%)
    pallas_call x1, Pallas kernels, body(): pl.pallas_call(functools.partial(kernel, n, tp, heads, latent_width, widt...  128 us

profile of v5, /device:TPU:0, one launch (start us, length us, event | category | flops | bytes accessed | tf_op | source)
XLA Modules:
  0.0 130.5 jit_solution(16599509790468347652)
XLA Ops:
  0.0 0.9 multiply_sine_fusion
  0.9 127.8 %shard_map.127 = bf16[96,2048]{1,0:T(8,128)(2,1)} custom-call(bf16[384,512]{1,0:T(8,128)(2,1)} %lat_ref.1, f32[1,512]{1,0:T(1,128)} %bitcast.14, bf16[64,384]{1,0:T(8,128)(2,1)} %bitcast.12, f32[32,384]{1,0:T(8,128)} %get-tuple-element.6.cos_ref, f32[32,384]{1,0:T(8,128)} %get-tuple-element.5.sin_ref, bf16[1536,128]{1,0:T(8,128)(2,1)} %bitcast.10, ...), custom_call_target="tpu_custom_call" | custom-call | tf_op jit(solution)/shard_map/pallas_call | solution.py:588
  128.7 1.8 %copy.15 = bf16[96,2048]{1,0:T(8,128)(2,1)} copy(bf16[96,2048]{1,0:T(8,128)(2,1)} %shard_map.127) | data formatting | bytes 786432
  (2 shorter events, 0.0 us)
